TPU v7x, 32 devices: a whole 2x2x4 slice. The times are simulated.
32 devices in a mesh: sp: 4 (over y, core), dp: 8 (over z, x).
Axes of the slice: x: 2, y: 2, z: 4, core: 2. Of those that a mesh axis runs over, the one named last changes fastest.
Arguments:
- q_latent: bfloat16 [8, 512, 512], P('dp', 'sp'), may hold values from -70 to 70
- kv_latent: bfloat16 [8, 512, 512], P('dp', 'sp'), may hold values from -70 to 70
- rope_key: bfloat16 [8, 512, 64], P('dp', 'sp'), may hold values from -370 to 370
- w_query: bfloat16 [512, 3072], P(None, 'dp'), may hold values from -0.25 to 0.25
- w_keyval: bfloat16 [512, 4096], P(None, 'sp'), may hold values from -0.25 to 0.25
- w_out: bfloat16 [2048, 2048], replicated, may hold values from -0.125 to 0.125
- query_gain: bfloat16 [512], replicated, may hold values from 0.099609375 to 1.8984375
- latent_gain: bfloat16 [512], replicated, may hold values from 0.099609375 to 1.8984375
- out_gain: bfloat16 [2048], replicated, may hold values from 0.099609375 to 1.8984375
Outputs:
- output: bfloat16 [8, 512, 2048], P('dp', 'sp')
All inputs are finite; a program needn't handle non-finite values.
Results may differ from a plain program's by a relative error of at most 0.03.
The roundings to bfloat16 on the way count: a program that leaves them out, or rounds other values in their place, can miss the bound.
Values may be sent and summed in bfloat16 or wider, within the bound.
A program may use at most 64 MiB of HBM per device.

v0:
```python
import functools

import jax
import jax.numpy as jnp
import numpy as np
from jax import lax
from jax.experimental import pallas as pl
from jax.experimental.pallas import tpu as pltpu
from jax.sharding import PartitionSpec as P

H = 16
NOPE = 128
ROPE = 64
VDIM = 128
HEAD = NOPE + ROPE
MESH = pl.DeviceIdType.MESH
F32 = jnp.float32
BF16 = jnp.bfloat16


def turn_table(length):
    half = ROPE // 2
    inverse = np.float32(10000.0) ** (-np.arange(half, dtype=np.float32) / np.float32(half))
    angles = np.arange(length, dtype=np.float32)[:, None] * inverse[None, :].astype(np.float32)
    angles = angles.astype(np.float64)
    cosine, sine = np.cos(angles), np.sin(angles)
    return np.concatenate([cosine, cosine, sine, sine], axis=1).astype(np.float32)


def spread_matrix(rows, row_start, head):
    g = lax.broadcasted_iota(jnp.int32, (rows, 256), 0) + row_start
    f = lax.broadcasted_iota(jnp.int32, (rows, 256), 1)
    source = jnp.where(f < HEAD, f, jnp.where(f < HEAD + 32, f - 32, f - 96)) + head * HEAD
    sign = jnp.where((f >= HEAD) & (f < HEAD + 32), -1.0, 1.0)
    return jnp.where(g == source, sign, 0.0).astype(BF16)


def rope_matrix():
    r = lax.broadcasted_iota(jnp.int32, (ROPE, 128), 0)
    f = lax.broadcasted_iota(jnp.int32, (ROPE, 128), 1)
    source = jnp.where(f < 64, f, jnp.where(f < 96, f - 32, f - 96))
    sign = jnp.where((f >= 64) & (f < 96), -1.0, 1.0)
    return jnp.where(r == source, sign, 0.0).astype(BF16)


def scaled_rows(values, gain):
    wide = values.astype(F32)
    mean = jnp.mean(wide * wide, axis=-1, keepdims=True)
    return (wide * lax.rsqrt(mean + 1e-05) * gain).astype(BF16)


def kernel(
    geometry,
    q_ref, kv_ref, rope_ref, wq_ref, wkv_ref, wout_ref, table_ref, qg_ref, lg_ref, og_ref,
    out_ref,
    qall, kvall, ropeall, wqall, wkv, wout, table, spread, qn, qs, ks, vs, att_out, att_in, acc,
    out_gain,
    local_sem, gat_send, gat_recv, fwd_send, w_send, w_recv, att_send, att_recv,
):
    n, m, X, k, chunks, local_heads, groups = geometry
    per_group = local_heads // groups
    width = wqall.shape[2]
    Z = m // X
    rows = q_ref.shape[1]
    n_chips = n // 2
    i = lax.axis_index("sp")
    j = lax.axis_index("dp")
    core = lax.rem(i, 2)
    chip = lax.div(i, 2)
    partner = i + 1 - 2 * core
    z = lax.div(j, X)
    x = lax.rem(j, X)
    first = i * k
    owns = (j >= first) & (j < first + k)

    gathered = ((kv_ref.at[0], kvall), (rope_ref.at[0], ropeall), (q_ref.at[0], qall))
    own_copies = [
        pltpu.make_async_copy(src, dst.at[i], local_sem.at[a]) for a, (src, dst) in enumerate(gathered)
    ]
    wq_copy = pltpu.make_async_copy(wq_ref, wqall.at[lax.rem(j, k)], local_sem.at[3])
    wkv_copy = pltpu.make_async_copy(wkv_ref, wkv, local_sem.at[4])
    table_copy = pltpu.make_async_copy(table_ref, table, local_sem.at[5])
    wout_copy = pltpu.make_async_copy(wout_ref, wout, local_sem.at[6])

    @pl.when(owns)
    def _():
        wq_copy.start()

    for copy in own_copies:
        copy.start()
    wkv_copy.start()
    table_copy.start()
    wout_copy.start()

    turner = rope_matrix()
    latent_gain = lg_ref[...].astype(F32).reshape(1, -1)
    query_gain = qg_ref[...].astype(F32).reshape(1, -1)
    group = local_heads * VDIM
    every_gain = og_ref[...].astype(F32).reshape(1, -1)
    for s in range(n):
        out_gain[s] = every_gain[:, s * group:(s + 1) * group]
    if groups > 1:
        for h in range(per_group):
            spread[h] = spread_matrix(width, 0, h)

    barrier = pltpu.get_barrier_semaphore()
    for d in range(1, n):
        pl.semaphore_signal(
            barrier, inc=1, device_id={"sp": lax.rem(i + d, n)}, device_id_type=MESH
        )
    sides = ((z < Z - 1, j + X), (z > 0, j - X), (x < X - 1, j + 1), (x > 0, j - 1))
    count = n - 1
    for present, target in sides:
        @pl.when(present)
        def _(target=target):
            pl.semaphore_signal(barrier, inc=1, device_id={"dp": target}, device_id_type=MESH)
        count = count + jnp.where(present, 1, 0)
    pl.semaphore_wait(barrier, count)

    step_rows = wqall.shape[1] // chunks

    def relay_parts(slot, c):
        owner = first + slot
        zo, xo = lax.div(owner, X), lax.rem(owner, X)
        part = wqall.at[slot, pl.ds(c * step_rows, step_rows)]
        in_column = x == xo
        conditions = (
            in_column & (z >= zo) & (z < Z - 1),
            in_column & (z <= zo) & (z > 0),
            (x >= xo) & (x < X - 1),
            (x <= xo) & (x > 0),
        )
        copies = [
            pltpu.make_async_remote_copy(
                src_ref=part, dst_ref=part,
                send_sem=w_send.at[side, slot, c], recv_sem=w_recv.at[slot, c],
                device_id={"dp": sides[side][1]}, device_id_type=MESH,
            )
            for side in range(4)
        ]
        return owner, conditions, copies

    def relay(slot, c):
        owner, conditions, copies = relay_parts(slot, c)

        @pl.when(owner != j)
        def _():
            copies[0].wait_recv()

        for condition, copy in zip(conditions, copies):
            @pl.when(condition)
            def _(copy=copy):
                copy.start()

    def relay_finish(slot, c):
        _, conditions, copies = relay_parts(slot, c)
        for condition, copy in zip(conditions, copies):
            @pl.when(condition)
            def _(copy=copy):
                copy.wait_send()

    if groups > 1:
        columns = [lax.rem(x + t, k) for t in range(k)]
        events = [[(column, c) for c in range(chunks)] for column in columns]
    else:
        columns = [0]
        events = [[(slot, c) for c in range(chunks) for slot in range(k)]]
    events_left = list(events[0])

    def relay_some(number):
        for _ in range(min(number, len(events_left))):
            relay(*events_left.pop(0))

    def gather_copy(a, slot, sem, target):
        dst = gathered[a][1]
        return pltpu.make_async_remote_copy(
            src_ref=dst.at[slot], dst_ref=dst.at[slot],
            send_sem=sem, recv_sem=gat_recv.at[a, slot],
            device_id={"sp": target}, device_id_type=MESH,
        )

    sends = []

    @pl.when(owns)
    def _():
        wq_copy.wait()

    for a in range(3):
        own_copies[a].wait()
        for d in range(1, n_chips):
            target = 2 * lax.rem(chip + d, n_chips) + core
            sends.append(gather_copy(a, i, gat_send.at[a, d], target))
            sends[-1].start()
    for a in range(3):
        sends.append(gather_copy(a, i, gat_send.at[a, 0], partner))
        sends[-1].start()

    def far_slot(d):
        return 2 * lax.rem(chip + n_chips - d, n_chips) + core

    def forward(a, d):
        slot = far_slot(d)
        copy = gather_copy(a, slot, fwd_send.at[a, d - 1], partner)
        copy.wait_recv()
        copy.start()
        sends.append(copy)

    def arrive(a, slot):
        gather_copy(a, slot, gat_send.at[a, 0], partner).wait_recv()

    lane = lax.broadcasted_iota(jnp.int32, (rows, 128), 1)

    def keyval(slot):
        at = pl.ds(pl.multiple_of(slot * rows, rows), rows)
        both = jnp.dot(
            scaled_rows(kvall[slot], latent_gain), wkv[...], preferred_element_type=F32
        ).astype(BF16)
        pair = lax.dot_general(
            ropeall[slot], turner, (((0,), (0,)), ((), ())), preferred_element_type=F32
        ) * table[at, :]
        pair = pair + pltpu.roll(pair, 64, 1)
        turned = jnp.where(lane < 64, pair, 0.0).astype(BF16)
        for h in range(local_heads):
            base = h * (NOPE + VDIM)
            ks[h, at, 0:NOPE] = both[:, base:base + NOPE]
            ks[h, at, NOPE:256] = turned
            vs[h, at, :] = both[:, base + NOPE:base + NOPE + VDIM]

    def query_rows(slot):
        at = pl.ds(pl.multiple_of(slot * rows, rows), rows)
        qn[at, :] = scaled_rows(qall[slot], query_gain)

    relay_some(k + 1)
    wkv_copy.wait()
    table_copy.wait()
    keyval(i)
    relay_some(1)
    query_rows(i)
    relay_some(1)
    arrive(0, partner)
    arrive(1, partner)
    keyval(partner)
    relay_some(1)
    for d in range(1, n_chips):
        forward(0, d)
        forward(1, d)
        keyval(far_slot(d))
        relay_some(1)
    arrive(2, partner)
    query_rows(partner)
    relay_some(2)
    for d in range(1, n_chips):
        other = far_slot(d) + 1 - 2 * core
        arrive(0, other)
        arrive(1, other)
        keyval(other)
        relay_some(2)
    for d in range(1, n_chips):
        forward(2, d)
        query_rows(far_slot(d))
        relay_some(2)
    for d in range(1, n_chips):
        other = far_slot(d) + 1 - 2 * core
        arrive(2, other)
        query_rows(other)
    relay_some(len(events_left))

    def raw_queries(slot, hh):
        if groups > 1:
            total = jnp.dot(wqall[slot], spread[hh], preferred_element_type=F32)
        else:
            total = None
            for s in range(k):
                if (s + 1) * width <= hh * HEAD or s * width >= (hh + 1) * HEAD:
                    continue
                term = jnp.dot(
                    wqall[s], spread_matrix(width, s * width, hh), preferred_element_type=F32
                )
                total = term if total is None else total + term
        return jnp.dot(qn[...], total.astype(BF16), preferred_element_type=F32)

    def queries(slot):
        for hh in range(per_group):
            h = slot * per_group + hh
            raw = raw_queries(slot, hh)
            qs[h, :, 0:NOPE] = raw[:, 0:NOPE].astype(BF16)
            pair = raw[:, NOPE:256] * table[...]
            qs[h, :, NOPE:256] = (pair + pltpu.roll(pair, 64, 1)).astype(BF16)

    power = HEAD ** (-0.5) * float(np.log2(np.e))
    causal = lax.broadcasted_iota(jnp.int32, (rows, rows), 1) <= lax.broadcasted_iota(
        jnp.int32, (rows, rows), 0
    )

    def attend(b, slot):
        stop = (b + 1) * rows
        for hh in range(per_group):
            h = slot * per_group + hh
            scores = lax.dot_general(
                qs[h, b * rows:stop, :], ks[h, 0:stop, :], (((1,), (1,)), ((), ())),
                preferred_element_type=F32,
            )
            last = jnp.where(causal, scores[:, b * rows:], -jnp.inf)
            if b:
                scores = jnp.concatenate([scores[:, :b * rows], last], axis=1)
            else:
                scores = last
            top = jnp.max(scores, axis=-1, keepdims=True)
            weights = jnp.exp2((scores - top) * power)
            row_total = jnp.sum(weights, axis=-1, keepdims=True)
            summed = jnp.dot(weights.astype(BF16), vs[h, 0:stop, :], preferred_element_type=F32)
            att_out[b, slot, :, hh * VDIM:(hh + 1) * VDIM] = (summed / row_total).astype(BF16)

    def att_copy(b, slot):
        return pltpu.make_async_remote_copy(
            src_ref=att_out.at[b, slot], dst_ref=att_in.at[i, slot],
            send_sem=att_send.at[b, slot], recv_sem=att_recv.at[i, slot],
            device_id={"sp": b}, device_id_type=MESH,
        )

    for t, slot in enumerate(columns):
        if t:
            for event in events[t]:
                relay(*event)
        queries(slot)
        for c in range(n_chips):
            @pl.when(chip != c)
            def _(c=c):
                for b in (2 * c, 2 * c + 1):
                    attend(b, slot)
                    att_copy(b, slot).start()
    for c in range(n_chips):
        @pl.when(chip == c)
        def _(c=c):
            for slot in columns:
                for b in (2 * c, 2 * c + 1):
                    attend(b, slot)
    for slot in columns:
        att_copy(partner, slot).start()

    wout_copy.wait()
    squares = None
    order = [partner]
    for d in range(1, n_chips):
        order += [far_slot(d), far_slot(d) + 1 - 2 * core]
    for t, s in enumerate([i] + order):
        source = att_out
        if t:
            source = att_in
            for slot in range(groups):
                pltpu.make_async_remote_copy(
                    src_ref=att_in.at[s, slot], dst_ref=att_in.at[s, slot],
                    send_sem=att_send.at[0, slot], recv_sem=att_recv.at[s, slot],
                    device_id={"sp": partner}, device_id_type=MESH,
                ).wait_recv()
        values = jnp.concatenate([source[s, slot] for slot in range(groups)], axis=1).astype(F32)
        at = pl.ds(pl.multiple_of(s * group, group), group)
        square = jnp.sum(values * values, axis=-1, keepdims=True)
        squares = square if squares is None else squares + square
        scaled = (values * out_gain[s]).astype(BF16)
        term = jnp.dot(scaled, wout[at, :], preferred_element_type=F32)
        if t == 0:
            acc[...] = term
        elif t < n - 1:
            acc[...] += term
        else:
            factor = lax.rsqrt(squares / (n * group) + 1e-05)
            out_ref[0] = ((acc[...] + term) * factor).astype(BF16)

    for copy in sends:
        copy.wait_send()
    for event in sum(events, []):
        relay_finish(*event)
    for b in range(n):
        @pl.when(i != b)
        def _(b=b):
            for slot in range(groups):
                att_copy(b, slot).wait_send()


def x_size(mesh):
    row = mesh.devices[0]
    places = [getattr(device, "coords", None) for device in row]
    if any(place is None for place in places):
        return 1
    return len({place[0] for place in places})


def per_device(
    mesh, q_latent, kv_latent, rope_key, w_query, w_keyval, w_out, query_gain, latent_gain, out_gain
):
    n, m = mesh.shape["sp"], mesh.shape["dp"]
    rows = q_latent.shape[1]
    length = n * rows
    rank = q_latent.shape[2]
    width = w_query.shape[1]
    local_heads = H // n
    k = local_heads * HEAD // width
    chunks = 16
    columns = x_size(mesh)
    groups = k if k == columns == 2 and width % HEAD == 0 else 1
    dim = w_out.shape[1]
    group = local_heads * VDIM
    table = jnp.asarray(turn_table(length))
    geometry = (n, m, columns, k, chunks, local_heads, groups)
    any_spec = pl.BlockSpec(memory_space=pl.ANY)
    vmem_spec = pl.BlockSpec(memory_space=pltpu.VMEM)
    dma = pltpu.SemaphoreType.DMA
    return pl.pallas_call(
        functools.partial(kernel, geometry),
        out_shape=jax.ShapeDtypeStruct((1, rows, dim), BF16),
        in_specs=[any_spec] * 7 + [vmem_spec] * 3,
        out_specs=vmem_spec,
        scratch_shapes=[
            pltpu.VMEM((n, rows, rank), BF16),
            pltpu.VMEM((n, rows, kv_latent.shape[2]), BF16),
            pltpu.VMEM((n, ROPE, rows), BF16),
            pltpu.VMEM((k, rank, width), BF16),
            pltpu.VMEM(w_keyval.shape, BF16),
            pltpu.VMEM(w_out.shape, BF16),
            pltpu.VMEM((length, 128), F32),
            pltpu.VMEM((local_heads // groups, width, 256), BF16),
            pltpu.VMEM((length, rank), BF16),
            pltpu.VMEM((local_heads, length, 256), BF16),
            pltpu.VMEM((local_heads, length, 256), BF16),
            pltpu.VMEM((local_heads, length, VDIM), BF16),
            pltpu.VMEM((n, groups, rows, group // groups), BF16),
            pltpu.VMEM((n, groups, rows, group // groups), BF16),
            pltpu.VMEM((rows, dim), F32),
            pltpu.VMEM((n, 1, group), F32),
            dma((7,)),
            dma((3, n // 2)),
            dma((3, n)),
            dma((3, n // 2)),
            dma((4, k, chunks)),
            dma((k, chunks)),
            dma((n, groups)),
            dma((n, groups)),
        ],
        compiler_params=pltpu.CompilerParams(
            collective_id=0, has_side_effects=True, vmem_limit_bytes=56 * 1024 * 1024
        ),
    )(
        q_latent, kv_latent, jnp.swapaxes(rope_key, 1, 2), w_query, w_keyval, w_out, table,
        query_gain, latent_gain, out_gain,
    )


def solution(mesh):
    in_specs = (
        P("dp", "sp", None),
        P("dp", "sp", None),
        P("dp", "sp", None),
        P(None, "dp"),
        P(None, "sp"),
        P(),
        P(),
        P(),
        P(),
    )
    return jax.shard_map(
        functools.partial(per_device, mesh), mesh=mesh, in_specs=in_specs,
        out_specs=P("dp", "sp", None), check_vma=False,
    )
```

profile of v0, /device:TPU:0, one launch (start us, length us, event | category | flops | bytes accessed | tf_op | source)
XLA Modules:
  0.0 37.4 jit_solution(13719510512092117200)
XLA Ops:
  0.0 35.5 %shard_map.100 = bf16[1,128,2048]{2,1,0:T(8,128)(2,1)} custom-call(bf16[1,128,512]{2,1,0:T(8,128)(2,1)} %q_ref.1, bf16[1,128,512]{2,1,0:T(8,128)(2,1)} %kv_ref.1, bf16[1,64,128]{2,1,0:T(8,128)(2,1)} %bitcast.1, bf16[512,384]{1,0:T(8,128)(2,1)} %wq_ref.1, bf16[512,1024]{1,0:T(8,128)(2,1)} %wkv_ref.1, bf16[2048,2048]{1,0:T(8,128)(2,1)} %wout_ref.1, ...), custom_call_target="tpu_custom_call" | custom-call | tf_op jit(solution)/shard_map/pallas_call | solution.py:409
  35.5 1.9 %copy.12 = bf16[1,128,2048]{2,1,0:T(8,128)(2,1)} copy(bf16[1,128,2048]{2,1,0:T(8,128)(2,1)} %shard_map.100) | data formatting | bytes 1048576
where the time goes:
time: 37.6 us; the launch traced here: 37.4 us
  Pallas kernels  35.5 us (94%)
  local copies, waits for them, and re-layouts  1.88 us (5%)
    pallas_call x1, Pallas kernels, per_device(): pl.pallas_call(functools.partial(kernel, geometry), out_shape=jax.ShapeDt...  35.5 us
    unnamed x1, local copies, waits for them, and re-layouts  1.88 us

commit v1 on v0

--- a/solution.py
+++ b/solution.py
@@ -408,7 +408,7 @@
     dma = pltpu.SemaphoreType.DMA
     return pl.pallas_call(
         functools.partial(kernel, geometry),
-        out_shape=jax.ShapeDtypeStruct((1, rows, dim), BF16),
+        out_shape=pltpu.VMEM((1, rows, dim), BF16),
         in_specs=[any_spec] * 7 + [vmem_spec] * 3,
         out_specs=vmem_spec,
         scratch_shapes=[

time: 37.6 us -> 35.7 us (0.949)
  local copies, waits for them, and re-layouts: 1.88 us -> 0.8 us
  Pallas kernels: 35.5 us -> 34.7 us
    unnamed x1, local copies, waits for them, and re-layouts: 1.88 us -> 0.8 us
    pallas_call x1, Pallas kernels: 35.5 us -> 34.7 us  [per_device(): pl.pallas_call(functools.partial(kernel, geometry), out_shape=pltpu.VMEM(...]
where the time goes in v1:
time: 35.7 us; the launch traced here: 35.5 us
  Pallas kernels  34.7 us (97%)
  local copies, waits for them, and re-layouts  0.8 us (2%)
    pallas_call x1, Pallas kernels, per_device(): pl.pallas_call(functools.partial(kernel, geometry), out_shape=pltpu.VMEM(...  34.7 us
    unnamed x1, local copies, waits for them, and re-layouts  0.8 us

profile of v1, /device:TPU:0, one launch (start us, length us, event | category | flops | bytes accessed | tf_op | source)
XLA Modules:
  0.0 35.5 jit_solution(7758863446118745291)
XLA Ops:
  0.0 34.7 %shard_map.100 = bf16[1,128,2048]{2,1,0:T(8,128)(2,1)S(1)} custom-call(bf16[1,128,512]{2,1,0:T(8,128)(2,1)} %q_ref.1, bf16[1,128,512]{2,1,0:T(8,128)(2,1)} %kv_ref.1, bf16[1,64,128]{2,1,0:T(8,128)(2,1)} %bitcast.1, bf16[512,384]{1,0:T(8,128)(2,1)} %wq_ref.1, bf16[512,1024]{1,0:T(8,128)(2,1)} %wkv_ref.1, bf16[2048,2048]{1,0:T(8,128)(2,1)} %wout_ref.1, ...), custom_call_target="tpu_custom_call" | custom-call | tf_op jit(solution)/shard_map/pallas_call | solution.py:409
  34.7 0.8 %copy.12 = bf16[1,128,2048]{2,1,0:T(8,128)(2,1)} copy(bf16[1,128,2048]{2,1,0:T(8,128)(2,1)S(1)} %shard_map.100) | data formatting | bytes 1048576

commit v2 on v1

--- a/solution.py
+++ b/solution.py
@@ -378,6 +378,424 @@
                 att_copy(b, slot).wait_send()
 
 
+def paired_table(length):
+    half = ROPE // 2
+    inverse = np.float32(10000.0) ** (-np.arange(half, dtype=np.float32) / np.float32(half))
+    angles = np.arange(length, dtype=np.float32)[:, None] * inverse[None, :].astype(np.float32)
+    angles = angles.astype(np.float64)
+    cosine, sine = np.cos(angles), np.sin(angles)
+    parts = [cosine] * 4 + [-sine, sine, -sine, sine]
+    return np.concatenate(parts, axis=1).astype(np.float32)
+
+
+def paired_kernel(
+    geometry,
+    q_ref, kv_ref, rope_ref, wq_ref, wkv_ref, wout_ref, table_ref, qg_ref, lg_ref, og_ref,
+    out_ref,
+    qall, kvall, ropeall, wqall, wkv, wout, table, qgain, lgain, ogain, qn, qs, ks, vs,
+    att_out, att_in, acc,
+    local_sem, gat_send, gat_recv, w_send, w_recv, x_recv, att_send, att_recv,
+):
+    n, X, Z, chunks, local_heads = geometry
+    width = wqall.shape[2]
+    rows = q_ref.shape[1]
+    n_chips = n // 2
+    i = lax.axis_index("sp")
+    j = lax.axis_index("dp")
+    core = lax.rem(i, 2)
+    chip = lax.div(i, 2)
+    partner = i + 1 - 2 * core
+    z = lax.div(j, X)
+    x = lax.rem(j, X)
+    across = 1 - x
+    zo = i
+    owns = z == zo
+    pair_dim = 2 * VDIM
+
+    gathered = ((kv_ref.at[0], kvall), (rope_ref.at[0], ropeall), (q_ref.at[0], qall))
+    own_copies = [
+        pltpu.make_async_copy(src, dst.at[i], local_sem.at[a]) for a, (src, dst) in enumerate(gathered)
+    ]
+    wq_copy = pltpu.make_async_copy(wq_ref, wqall.at[x], local_sem.at[3])
+    wkv_copy = pltpu.make_async_copy(wkv_ref, wkv, local_sem.at[4])
+    table_copy = pltpu.make_async_copy(table_ref, table, local_sem.at[5])
+    wout_copy = pltpu.make_async_copy(wout_ref, wout, local_sem.at[6])
+    gain_copies = [
+        pltpu.make_async_copy(src, dst, local_sem.at[7 + a])
+        for a, (src, dst) in enumerate(((qg_ref, qgain), (lg_ref, lgain), (og_ref, ogain)))
+    ]
+
+    barrier = pltpu.get_barrier_semaphore()
+    for d in range(1, n):
+        pl.semaphore_signal(
+            barrier, inc=1, device_id={"sp": lax.rem(i + d, n)}, device_id_type=MESH
+        )
+    low_end = zo == 0
+    high_end = zo == Z - 1
+    greet = (
+        (z < Z - 1, j + X), (z > 0, j - X), (x >= 0, j + 1 - 2 * x),
+        (low_end & (z == 0), j + 2 * X), (low_end & (z == 2), j - 2 * X),
+        (high_end & (z == Z - 1), j - 2 * X), (high_end & (z == Z - 3), j + 2 * X),
+    )
+    count = n - 1
+    for present, target in greet:
+        @pl.when(present)
+        def _(target=target):
+            pl.semaphore_signal(barrier, inc=1, device_id={"dp": target}, device_id_type=MESH)
+        count = count + jnp.where(present, 1, 0)
+
+    @pl.when(owns)
+    def _():
+        wq_copy.start()
+
+    for copy in own_copies:
+        copy.start()
+    for copy in gain_copies:
+        copy.start()
+    wkv_copy.start()
+    table_copy.start()
+    wout_copy.start()
+
+    for h in range(local_heads):
+        vs[h, :, VDIM:2 * VDIM] = jnp.ones((vs.shape[1], VDIM), BF16)
+    r = lax.broadcasted_iota(jnp.int32, (ROPE, 128), 0)
+    f = lax.broadcasted_iota(jnp.int32, (ROPE, 128), 1)
+    turner = jnp.where(r == lax.rem(f, ROPE), 1.0, 0.0).astype(BF16)
+
+    step_rows = wqall.shape[1] // chunks
+
+    def w_part(c):
+        return wqall.at[x, pl.ds(c * step_rows, step_rows)]
+
+    sides = (
+        ((z >= zo) & (z < Z - 1) & jnp.logical_not(low_end & (z == 1)), j + X),
+        ((z <= zo) & (z > 0) & jnp.logical_not(high_end & (z == Z - 2)), j - X),
+        (low_end & (z == 0), j + 2 * X),
+        (high_end & (z == Z - 1), j - 2 * X),
+    )
+
+    def w_copy(side, c):
+        part = w_part(c)
+        return pltpu.make_async_remote_copy(
+            src_ref=part, dst_ref=part, send_sem=w_send.at[side], recv_sem=w_recv.at[c],
+            device_id={"dp": sides[side][1]}, device_id_type=MESH,
+        )
+
+    def x_copy(part):
+        return pltpu.make_async_remote_copy(
+            src_ref=part, dst_ref=part, send_sem=w_send.at[4], recv_sem=x_recv.at[0],
+            device_id={"dp": j + 1 - 2 * x}, device_id_type=MESH,
+        )
+
+    chunks_left = list(range(chunks))
+
+    def relay(number):
+        number = min(number, len(chunks_left))
+        if not number:
+            return
+        todo = [chunks_left.pop(0) for _ in range(number)]
+
+        @pl.when(jnp.logical_not(owns))
+        def _():
+            for c in todo:
+                w_copy(0, c).wait_recv()
+                for side in (0, 1):
+                    @pl.when(sides[side][0])
+                    def _(side=side, c=c):
+                        w_copy(side, c).start()
+                x_copy(w_part(c)).start()
+
+    def gather_copy(a, slot, target):
+        dst = gathered[a][1]
+        return pltpu.make_async_remote_copy(
+            src_ref=dst.at[slot], dst_ref=dst.at[slot],
+            send_sem=gat_send.at[a], recv_sem=gat_recv.at[a, slot],
+            device_id={"sp": target}, device_id_type=MESH,
+        )
+
+    def far_slot(d):
+        return 2 * lax.rem(chip + n_chips - d, n_chips) + core
+
+    def forward(a, d):
+        slot = far_slot(d)
+        copy = gather_copy(a, slot, partner)
+        copy.wait_recv()
+        copy.start()
+
+    def arrive(a, slot):
+        gather_copy(a, slot, partner).wait_recv()
+
+    lane = lax.broadcasted_iota(jnp.int32, (rows, 128), 1)
+    left = lane < 64
+
+    def turned_pair(both_halves, at):
+        swap_low = lax.rem(lax.broadcasted_iota(jnp.int32, both_halves.shape, 1), 64) < 32
+        swapped = jnp.where(
+            swap_low, pltpu.roll(both_halves, 96, 1), pltpu.roll(both_halves, 32, 1)
+        )
+        return both_halves * table[at, 0:128] + swapped * table[at, 128:256]
+
+    def keyval(slot):
+        at = pl.ds(pl.multiple_of(slot * rows, rows), rows)
+        both = jnp.dot(
+            scaled_rows(kvall[slot], lgain[...].astype(F32).reshape(1, -1)), wkv[...],
+            preferred_element_type=F32,
+        )
+        twice = lax.dot_general(
+            ropeall[slot], turner, (((0,), (0,)), ((), ())), preferred_element_type=F32
+        )
+        turned = turned_pair(twice, at)
+        for h in range(local_heads):
+            base = h * (NOPE + VDIM)
+            key = both[:, base:base + NOPE]
+            if h % 2 == 0:
+                ks[h, at, 0:NOPE] = key.astype(BF16)
+                ks[h, at, NOPE:256] = jnp.where(left, turned, 0.0).astype(BF16)
+            else:
+                key = pltpu.roll(key, 64, 1)
+                ks[h, at, 0:NOPE] = jnp.where(left, 0.0, key).astype(BF16)
+                ks[h, at, NOPE:256] = jnp.where(left, key, turned).astype(BF16)
+            vs[h, at, 0:VDIM] = both[:, base + NOPE:base + NOPE + VDIM].astype(BF16)
+
+    def query_rows(slot):
+        at = pl.ds(pl.multiple_of(slot * rows, rows), rows)
+        qn[at, :] = scaled_rows(qall[slot], qgain[...].astype(F32).reshape(1, -1))
+
+    for copy in own_copies:
+        copy.wait()
+    for copy in gain_copies:
+        copy.wait()
+    query_rows(i)
+
+    @pl.when(owns)
+    def _():
+        wq_copy.wait()
+
+    pl.semaphore_wait(barrier, count)
+
+    for a in range(3):
+        for d in range(1, n_chips):
+            gather_copy(a, i, 2 * lax.rem(chip + d, n_chips) + core).start()
+
+    @pl.when(owns)
+    def _():
+        x_copy(wqall.at[x]).start()
+        for c in range(chunks):
+            for side in range(4):
+                @pl.when(sides[side][0])
+                def _(side=side, c=c):
+                    w_copy(side, c).start()
+
+    for a in range(3):
+        gather_copy(a, i, partner).start()
+
+    wkv_copy.wait()
+    table_copy.wait()
+    keyval(i)
+    arrive(0, partner)
+    arrive(1, partner)
+    keyval(partner)
+    arrive(2, partner)
+    query_rows(partner)
+    relay(chunks * 3 // 8)
+    for d in range(1, n_chips):
+        forward(0, d)
+        forward(1, d)
+        relay(chunks // 16)
+        keyval(far_slot(d))
+        relay(chunks // 16)
+    for d in range(1, n_chips):
+        other = far_slot(d) + 1 - 2 * core
+        arrive(0, other)
+        arrive(1, other)
+        keyval(other)
+        relay(chunks // 8)
+    for d in range(1, n_chips):
+        forward(2, d)
+        query_rows(far_slot(d))
+        relay(chunks // 8)
+    for d in range(1, n_chips):
+        other = far_slot(d) + 1 - 2 * core
+        arrive(2, other)
+        query_rows(other)
+    relay(len(chunks_left))
+
+    wide = (qn.shape[0], 128)
+    wide_left = lax.broadcasted_iota(jnp.int32, wide, 1) < 64
+
+    def queries(slot):
+        raw = jnp.dot(qn[...], wqall[slot], preferred_element_type=F32)
+        mid, last = raw[:, 128:256], raw[:, 256:384]
+        turned = turned_pair(jnp.where(wide_left, mid, last), pl.ds(0, qn.shape[0]))
+        qs[slot, :, 0:128] = raw[:, 0:128].astype(BF16)
+        qs[slot, :, 128:256] = jnp.where(wide_left, turned, mid).astype(BF16)
+        qs[slot, :, 256:384] = jnp.where(wide_left, last, turned).astype(BF16)
+
+    power = HEAD ** (-0.5) * float(np.log2(np.e))
+    block = 2 * rows
+    causal = lax.broadcasted_iota(jnp.int32, (block, block), 1) <= lax.broadcasted_iota(
+        jnp.int32, (block, block), 0
+    )
+
+    def attend(c, slot):
+        start, stop = c * block, (c + 1) * block
+        scores = []
+        for hh in range(2):
+            score = lax.dot_general(
+                qs[slot, start:stop, hh * 128:hh * 128 + 256], ks[2 * slot + hh, 0:stop, :],
+                (((1,), (1,)), ((), ())), preferred_element_type=F32,
+            )
+            last = jnp.where(causal, score[:, start:], -jnp.inf)
+            scores.append(jnp.concatenate([score[:, :start], last], axis=1) if c else last)
+        tops = [jnp.max(score, axis=-1, keepdims=True) for score in scores]
+        weights = [
+            jnp.exp2((score - top) * power).astype(BF16) for score, top in zip(scores, tops)
+        ]
+        for hh in range(2):
+            summed = jnp.dot(
+                weights[hh], vs[2 * slot + hh, 0:stop, :], preferred_element_type=F32
+            )
+            result = (summed[:, 0:VDIM] / summed[:, VDIM:2 * VDIM]).astype(BF16)
+            for e in range(2):
+                att_out[2 * c + e, slot, :, hh * VDIM:(hh + 1) * VDIM] = result[
+                    e * rows:(e + 1) * rows
+                ]
+
+    def att_copy(b, slot):
+        return pltpu.make_async_remote_copy(
+            src_ref=att_out.at[b, slot], dst_ref=att_in.at[i, slot],
+            send_sem=att_send.at[0], recv_sem=att_recv.at[i, slot],
+            device_id={"sp": b}, device_id_type=MESH,
+        )
+
+    for t, slot in enumerate((x, across)):
+        if t:
+            x_copy(wqall.at[across]).wait_recv()
+        queries(slot)
+        for c in range(n_chips):
+            @pl.when(chip != c)
+            def _(c=c):
+                attend(c, slot)
+                for b in (2 * c, 2 * c + 1):
+                    att_copy(b, slot).start()
+    for slot in (x, across):
+        for c in range(n_chips):
+            @pl.when(chip == c)
+            def _(c=c):
+                attend(c, slot)
+        att_copy(partner, slot).start()
+
+    wout_copy.wait()
+    squares = []
+    group = 2 * pair_dim
+
+    def piece(s, slot, local):
+        if not local:
+            pltpu.make_async_remote_copy(
+                src_ref=att_in.at[s, slot], dst_ref=att_in.at[s, slot],
+                send_sem=att_send.at[0], recv_sem=att_recv.at[s, slot],
+                device_id={"sp": partner}, device_id_type=MESH,
+            ).wait_recv()
+        values = (att_out if local else att_in)[s, slot].astype(F32)
+        squares.append(jnp.sum(values * values, axis=-1, keepdims=True))
+        at = pl.multiple_of(s * group + slot * pair_dim, pair_dim)
+        gain = ogain[pl.ds(at, pair_dim)].astype(F32).reshape(1, -1)
+        return jnp.dot(
+            (values * gain).astype(BF16), wout[pl.ds(at, pair_dim), :],
+            preferred_element_type=F32,
+        )
+
+    acc[...] = piece(i, x, True) + piece(i, across, True)
+    acc[...] += piece(partner, x, False) + piece(partner, across, False)
+    far = []
+    for d in range(1, n_chips):
+        far += [far_slot(d), far_slot(d) + 1 - 2 * core]
+    steps = [(s, slot) for slot in (x, across) for s in far]
+    for s, slot in steps[:-1]:
+        acc[...] += piece(s, slot, False)
+    term = piece(*steps[-1], False)
+    factor = lax.rsqrt(sum(squares[1:], squares[0]) / (n * group) + 1e-05)
+    out_ref[0] = ((acc[...] + term) * factor).astype(BF16)
+
+    for a in range(3):
+        every = gathered[a][1].at[pl.ds(0, n - 1)]
+        pltpu.make_async_remote_copy(
+            src_ref=every, dst_ref=every, send_sem=gat_send.at[a], recv_sem=gat_recv.at[a, 0],
+            device_id={"sp": partner}, device_id_type=MESH,
+        ).wait_send()
+    for side in range(4):
+        @pl.when(sides[side][0])
+        def _(side=side):
+            pltpu.make_async_remote_copy(
+                src_ref=wqall.at[x], dst_ref=wqall.at[x],
+                send_sem=w_send.at[side], recv_sem=w_recv.at[0],
+                device_id={"dp": sides[side][1]}, device_id_type=MESH,
+            ).wait_send()
+    x_copy(wqall.at[x]).wait_send()
+    every = att_out.at[pl.ds(0, n - 1)]
+    pltpu.make_async_remote_copy(
+        src_ref=every, dst_ref=every, send_sem=att_send.at[0], recv_sem=att_recv.at[0, 0],
+        device_id={"sp": partner}, device_id_type=MESH,
+    ).wait_send()
+
+
+def paired(
+    mesh, columns, q_latent, kv_latent, rope_key, w_query, w_keyval, w_out, query_gain, latent_gain,
+    out_gain,
+):
+    n, m = mesh.shape["sp"], mesh.shape["dp"]
+    rows = q_latent.shape[1]
+    length = n * rows
+    rank = q_latent.shape[2]
+    width = w_query.shape[1]
+    local_heads = H // n
+    chunks = 16
+    dim = w_out.shape[1]
+    geometry = (n, columns, m // columns, chunks, local_heads)
+    any_spec = pl.BlockSpec(memory_space=pl.ANY)
+    vmem_spec = pl.BlockSpec(memory_space=pltpu.VMEM)
+    dma = pltpu.SemaphoreType.DMA
+    return pl.pallas_call(
+        functools.partial(paired_kernel, geometry),
+        out_shape=pltpu.VMEM((1, rows, dim), BF16),
+        in_specs=[any_spec] * 10,
+        out_specs=vmem_spec,
+        scratch_shapes=[
+            pltpu.VMEM((n, rows, rank), BF16),
+            pltpu.VMEM((n, rows, kv_latent.shape[2]), BF16),
+            pltpu.VMEM((n, ROPE, rows), BF16),
+            pltpu.VMEM((columns, rank, width), BF16),
+            pltpu.VMEM(w_keyval.shape, BF16),
+            pltpu.VMEM(w_out.shape, BF16),
+            pltpu.VMEM((length, 256), F32),
+            pltpu.VMEM(query_gain.shape, BF16),
+            pltpu.VMEM(latent_gain.shape, BF16),
+            pltpu.VMEM(out_gain.shape, BF16),
+            pltpu.VMEM((length, rank), BF16),
+            pltpu.VMEM((columns, length, width), BF16),
+            pltpu.VMEM((local_heads, length, 256), BF16),
+            pltpu.VMEM((local_heads, length, 2 * VDIM), BF16),
+            pltpu.VMEM((n, columns, rows, 2 * VDIM), BF16),
+            pltpu.VMEM((n, columns, rows, 2 * VDIM), BF16),
+            pltpu.VMEM((rows, dim), F32),
+            dma((10,)),
+            dma((3,)),
+            dma((3, n)),
+            dma((5,)),
+            dma((chunks,)),
+            dma((1,)),
+            dma((1,)),
+            dma((n, columns)),
+        ],
+        compiler_params=pltpu.CompilerParams(
+            collective_id=0, has_side_effects=True, vmem_limit_bytes=56 * 1024 * 1024
+        ),
+    )(
+        q_latent, kv_latent, jnp.swapaxes(rope_key, 1, 2), w_query, w_keyval, w_out,
+        jnp.asarray(paired_table(length)), query_gain, latent_gain, out_gain,
+    )
+
+
 def x_size(mesh):
     row = mesh.devices[0]
     places = [getattr(device, "coords", None) for device in row]
@@ -401,6 +819,11 @@
     groups = k if k == columns == 2 and width % HEAD == 0 else 1
     dim = w_out.shape[1]
     group = local_heads * VDIM
+    if groups == columns and width == 2 * HEAD and H % m == 0 and m == n * columns:
+        return paired(
+            mesh, columns, q_latent, kv_latent, rope_key, w_query, w_keyval, w_out, query_gain,
+            latent_gain, out_gain,
+        )
     table = jnp.asarray(turn_table(length))
     geometry = (n, m, columns, k, chunks, local_heads, groups)
     any_spec = pl.BlockSpec(memory_space=pl.ANY)

time: 35.7 us -> 28.5 us (0.80)
  Pallas kernels: 34.7 us -> 27.6 us
    pallas_call x1, Pallas kernels: 34.7 us -> 27.6 us  [paired(): pl.pallas_call(functools.partial(paired_kernel, geometry), out_shape=pltp...]
where the time goes in v2:
time: 28.5 us; the launch traced here: 28.4 us
  Pallas kernels  27.6 us (97%)
  local copies, waits for them, and re-layouts  0.8 us (3%)
    pallas_call x1, Pallas kernels, paired(): pl.pallas_call(functools.partial(paired_kernel, geometry), out_shape=pltp...  27.6 us
    unnamed x1, local copies, waits for them, and re-layouts  0.8 us

profile of v2, /device:TPU:0, one launch (start us, length us, event | category | flops | bytes accessed | tf_op | source)
XLA Modules:
  0.0 28.4 jit_solution(987995633634352273)
XLA Ops:
  0.0 27.6 %shard_map.100 = bf16[1,128,2048]{2,1,0:T(8,128)(2,1)S(1)} custom-call(bf16[1,128,512]{2,1,0:T(8,128)(2,1)} %q_ref.1, bf16[1,128,512]{2,1,0:T(8,128)(2,1)} %kv_ref.1, bf16[1,64,128]{2,1,0:T(8,128)(2,1)} %bitcast.1, bf16[512,384]{1,0:T(8,128)(2,1)} %wq_ref.1, bf16[512,1024]{1,0:T(8,128)(2,1)} %wkv_ref.1, bf16[2048,2048]{1,0:T(8,128)(2,1)} %wout_ref.1, ...), custom_call_target="tpu_custom_call" | custom-call | tf_op jit(solution)/shard_map/pallas_call | solution.py:758
  27.6 0.8 %copy.12 = bf16[1,128,2048]{2,1,0:T(8,128)(2,1)} copy(bf16[1,128,2048]{2,1,0:T(8,128)(2,1)S(1)} %shard_map.100) | data formatting | bytes 1048576

commit v3 on v2

--- a/solution.py
+++ b/solution.py
@@ -392,12 +392,13 @@
     geometry,
     q_ref, kv_ref, rope_ref, wq_ref, wkv_ref, wout_ref, table_ref, qg_ref, lg_ref, og_ref,
     out_ref,
-    qall, kvall, ropeall, wqall, wkv, wout, table, qgain, lgain, ogain, qn, qs, ks, vs,
+    qall, kvall, ropeall, wqa, wqb, assist, wkv, wout, table, qgain, lgain, ogain, head_gain, qn, qs, ks, vs,
     att_out, att_in, acc,
     local_sem, gat_send, gat_recv, w_send, w_recv, x_recv, att_send, att_recv,
 ):
     n, X, Z, chunks, local_heads = geometry
-    width = wqall.shape[2]
+    whead = (wqa, wqb)
+    first_width = wqa.shape[2]
     rows = q_ref.shape[1]
     n_chips = n // 2
     i = lax.axis_index("sp")
@@ -410,13 +411,17 @@
     across = 1 - x
     zo = i
     owns = z == zo
-    pair_dim = 2 * VDIM
 
     gathered = ((kv_ref.at[0], kvall), (rope_ref.at[0], ropeall), (q_ref.at[0], qall))
     own_copies = [
         pltpu.make_async_copy(src, dst.at[i], local_sem.at[a]) for a, (src, dst) in enumerate(gathered)
     ]
-    wq_copy = pltpu.make_async_copy(wq_ref, wqall.at[x], local_sem.at[3])
+    wq_copies = [
+        pltpu.make_async_copy(wq_ref.at[:, 0:first_width], wqa.at[x], local_sem.at[3]),
+        pltpu.make_async_copy(
+            wq_ref.at[:, first_width:first_width + wqb.shape[2]], wqb.at[x], local_sem.at[10]
+        ),
+    ]
     wkv_copy = pltpu.make_async_copy(wkv_ref, wkv, local_sem.at[4])
     table_copy = pltpu.make_async_copy(table_ref, table, local_sem.at[5])
     wout_copy = pltpu.make_async_copy(wout_ref, wout, local_sem.at[6])
@@ -425,28 +430,50 @@
         for a, (src, dst) in enumerate(((qg_ref, qgain), (lg_ref, lgain), (og_ref, ogain)))
     ]
 
+    assist_copy = pltpu.make_async_copy(
+        wq_ref.at[:, first_width:first_width + wqb.shape[2]], assist, local_sem.at[11]
+    )
+
     barrier = pltpu.get_barrier_semaphore()
     for d in range(1, n):
         pl.semaphore_signal(
             barrier, inc=1, device_id={"sp": lax.rem(i + d, n)}, device_id_type=MESH
         )
-    low_end = zo == 0
-    high_end = zo == Z - 1
+    def places(owner):
+        low = owner * 2 < Z
+        inner = owner == jnp.where(low, 1, Z - 2)
+        last = jnp.where(low, Z - 1, 0)
+        relayer = jnp.where(low, Z - 2, 1)
+        return last, relayer, jnp.where(low, jnp.where(inner, 0, 1), jnp.where(inner, Z - 1, Z - 2))
+
+    end, mid, other = places(zo)
+    at_mid, at_end, at_other = z == mid, z == end, z == other
+    twin = lax.rem(i + n // 2, n)
+    twin_end = places(twin)[0]
+    assists = z == twin
+
+    def row(target, column=x):
+        return target * X + column
+
     greet = (
-        (z < Z - 1, j + X), (z > 0, j - X), (x >= 0, j + 1 - 2 * x),
-        (low_end & (z == 0), j + 2 * X), (low_end & (z == 2), j - 2 * X),
-        (high_end & (z == Z - 1), j - 2 * X), (high_end & (z == Z - 3), j + 2 * X),
+        (at_other | at_mid, {"dp": row(zo)}), (at_end, {"dp": row(mid)}),
+        (at_end, {"sp": twin, "dp": row(zo)}), (at_end, {"sp": twin, "dp": row(zo, across)}),
     )
-    count = n - 1
+    pl.semaphore_signal(barrier, inc=1, device_id={"dp": row(z, across)}, device_id_type=MESH)
+    count = n + jnp.where(owns, 2, 0) + jnp.where(at_mid, 1, 0) + jnp.where(assists, 2, 0)
     for present, target in greet:
         @pl.when(present)
         def _(target=target):
-            pl.semaphore_signal(barrier, inc=1, device_id={"dp": target}, device_id_type=MESH)
-        count = count + jnp.where(present, 1, 0)
+            pl.semaphore_signal(barrier, inc=1, device_id=target, device_id_type=MESH)
+
+    @pl.when(assists)
+    def _():
+        assist_copy.start()
 
     @pl.when(owns)
     def _():
-        wq_copy.start()
+        for copy in wq_copies:
+            copy.start()
 
     for copy in own_copies:
         copy.start()
@@ -462,48 +489,58 @@
     f = lax.broadcasted_iota(jnp.int32, (ROPE, 128), 1)
     turner = jnp.where(r == lax.rem(f, ROPE), 1.0, 0.0).astype(BF16)
 
-    step_rows = wqall.shape[1] // chunks
-
-    def w_part(c):
-        return wqall.at[x, pl.ds(c * step_rows, step_rows)]
-
-    sides = (
-        ((z >= zo) & (z < Z - 1) & jnp.logical_not(low_end & (z == 1)), j + X),
-        ((z <= zo) & (z > 0) & jnp.logical_not(high_end & (z == Z - 2)), j - X),
-        (low_end & (z == 0), j + 2 * X),
-        (high_end & (z == Z - 1), j - 2 * X),
-    )
+    parts = [(part, c) for part in range(2) for c in range(chunks[part])]
+
+    def w_part(index):
+        part, c = parts[index]
+        step = whead[part].shape[1] // chunks[part]
+        return whead[part].at[x, pl.ds(c * step, step)]
+
+    targets = (row(other), row(mid), row(end))
+
+    def assist_send(column, sem):
+        return pltpu.make_async_remote_copy(
+            src_ref=assist, dst_ref=wqb.at[x], send_sem=w_send.at[10 + sem],
+            recv_sem=x_recv.at[1 + sem],
+            device_id={"sp": twin, "dp": row(twin_end, column)}, device_id_type=MESH,
+        )
 
     def w_copy(side, c):
         part = w_part(c)
         return pltpu.make_async_remote_copy(
-            src_ref=part, dst_ref=part, send_sem=w_send.at[side], recv_sem=w_recv.at[c],
-            device_id={"dp": sides[side][1]}, device_id_type=MESH,
-        )
-
-    def x_copy(part):
+            src_ref=part, dst_ref=part, send_sem=w_send.at[4 * parts[c][0] + side], recv_sem=w_recv.at[c],
+            device_id={"dp": targets[side]}, device_id_type=MESH,
+        )
+
+    def x_copy(source, part):
         return pltpu.make_async_remote_copy(
-            src_ref=part, dst_ref=part, send_sem=w_send.at[4], recv_sem=x_recv.at[0],
+            src_ref=source, dst_ref=source, send_sem=w_send.at[8 + part], recv_sem=x_recv.at[part],
             device_id={"dp": j + 1 - 2 * x}, device_id_type=MESH,
         )
 
-    chunks_left = list(range(chunks))
-
-    def relay(number):
-        number = min(number, len(chunks_left))
-        if not number:
-            return
-        todo = [chunks_left.pop(0) for _ in range(number)]
-
-        @pl.when(jnp.logical_not(owns))
-        def _():
-            for c in todo:
-                w_copy(0, c).wait_recv()
-                for side in (0, 1):
-                    @pl.when(sides[side][0])
-                    def _(side=side, c=c):
-                        w_copy(side, c).start()
-                x_copy(w_part(c)).start()
+    late = at_end
+    soon = at_mid | at_other
+    chunks_left = {True: list(range(len(parts))), False: list(range(len(parts)))}
+
+    def relay_one(index):
+        w_copy(0, index).wait_recv()
+        if parts[index][0] == 0:
+            @pl.when(at_mid)
+            def _():
+                w_copy(2, index).start()
+        x_copy(w_part(index), parts[index][0]).start()
+
+    chunks_left[True] = chunks_left[True][:chunks[0]]
+
+    def relay(early, after):
+        for is_late, number in ((False, early), (True, after)):
+            left = chunks_left[is_late]
+            todo = [left.pop(0) for _ in range(min(number, len(left)))]
+            if todo:
+                @pl.when(late if is_late else soon)
+                def _(todo=todo):
+                    for index in todo:
+                        relay_one(index)
 
     def gather_copy(a, slot, target):
         dst = gathered[a][1]
@@ -566,10 +603,14 @@
     for copy in gain_copies:
         copy.wait()
     query_rows(i)
+    every_gain = ogain[...].astype(F32).reshape(1, -1)
+    for h in range(n * local_heads):
+        head_gain[h] = every_gain[:, h * VDIM:(h + 1) * VDIM]
 
     @pl.when(owns)
     def _():
-        wq_copy.wait()
+        for copy in wq_copies:
+            copy.wait()
 
     pl.semaphore_wait(barrier, count)
 
@@ -579,12 +620,11 @@
 
     @pl.when(owns)
     def _():
-        x_copy(wqall.at[x]).start()
-        for c in range(chunks):
-            for side in range(4):
-                @pl.when(sides[side][0])
-                def _(side=side, c=c):
-                    w_copy(side, c).start()
+        for part in range(2):
+            x_copy(whead[part].at[x], part).start()
+        for index in range(len(parts)):
+            w_copy(1, index).start()
+            w_copy(0, index).start()
 
     for a in range(3):
         gather_copy(a, i, partner).start()
@@ -597,39 +637,50 @@
     keyval(partner)
     arrive(2, partner)
     query_rows(partner)
-    relay(chunks * 3 // 8)
+    relay(4, 0)
     for d in range(1, n_chips):
         forward(0, d)
         forward(1, d)
-        relay(chunks // 16)
+        relay(1, 0)
         keyval(far_slot(d))
-        relay(chunks // 16)
+    @pl.when(assists)
+    def _():
+        assist_copy.wait()
+        assist_send(x, 1).start()
+
+    relay(1, 1)
     for d in range(1, n_chips):
         other = far_slot(d) + 1 - 2 * core
         arrive(0, other)
         arrive(1, other)
         keyval(other)
-        relay(chunks // 8)
+    @pl.when(assists)
+    def _():
+        assist_send(across, 0).start()
+
+    relay(1, 2)
     for d in range(1, n_chips):
         forward(2, d)
         query_rows(far_slot(d))
-        relay(chunks // 8)
+    relay(1, 1)
     for d in range(1, n_chips):
         other = far_slot(d) + 1 - 2 * core
         arrive(2, other)
         query_rows(other)
-    relay(len(chunks_left))
+    relay(1, 5)
 
     wide = (qn.shape[0], 128)
     wide_left = lax.broadcasted_iota(jnp.int32, wide, 1) < 64
 
-    def queries(slot):
-        raw = jnp.dot(qn[...], wqall[slot], preferred_element_type=F32)
-        mid, last = raw[:, 128:256], raw[:, 256:384]
-        turned = turned_pair(jnp.where(wide_left, mid, last), pl.ds(0, qn.shape[0]))
-        qs[slot, :, 0:128] = raw[:, 0:128].astype(BF16)
-        qs[slot, :, 128:256] = jnp.where(wide_left, turned, mid).astype(BF16)
-        qs[slot, :, 256:384] = jnp.where(wide_left, last, turned).astype(BF16)
+    def queries(slot, part):
+        raw = jnp.dot(qn[...], whead[part][slot], preferred_element_type=F32)
+        last = raw[:, raw.shape[1] - 128:]
+        turned = turned_pair(last, pl.ds(0, qn.shape[0]))
+        if part == 0:
+            qs[slot, :, 0:128] = raw[:, 0:128].astype(BF16)
+            qs[slot, :, 128:256] = jnp.where(wide_left, turned, last).astype(BF16)
+        else:
+            qs[slot, :, 256:384] = jnp.where(wide_left, last, turned).astype(BF16)
 
     power = HEAD ** (-0.5) * float(np.log2(np.e))
     block = 2 * rows
@@ -637,10 +688,10 @@
         jnp.int32, (block, block), 0
     )
 
-    def attend(c, slot):
+    def attend(c, slot, heads):
         start, stop = c * block, (c + 1) * block
         scores = []
-        for hh in range(2):
+        for hh in heads:
             score = lax.dot_general(
                 qs[slot, start:stop, hh * 128:hh * 128 + 256], ks[2 * slot + hh, 0:stop, :],
                 (((1,), (1,)), ((), ())), preferred_element_type=F32,
@@ -651,68 +702,87 @@
         weights = [
             jnp.exp2((score - top) * power).astype(BF16) for score, top in zip(scores, tops)
         ]
-        for hh in range(2):
-            summed = jnp.dot(
-                weights[hh], vs[2 * slot + hh, 0:stop, :], preferred_element_type=F32
-            )
+        for hh, weight in zip(heads, weights):
+            summed = jnp.dot(weight, vs[2 * slot + hh, 0:stop, :], preferred_element_type=F32)
             result = (summed[:, 0:VDIM] / summed[:, VDIM:2 * VDIM]).astype(BF16)
             for e in range(2):
-                att_out[2 * c + e, slot, :, hh * VDIM:(hh + 1) * VDIM] = result[
-                    e * rows:(e + 1) * rows
-                ]
-
-    def att_copy(b, slot):
+                att_out[2 * c + e, 2 * slot + hh] = result[e * rows:(e + 1) * rows]
+
+    def att_copy(b, head):
         return pltpu.make_async_remote_copy(
-            src_ref=att_out.at[b, slot], dst_ref=att_in.at[i, slot],
-            send_sem=att_send.at[0], recv_sem=att_recv.at[i, slot],
+            src_ref=att_out.at[b, head], dst_ref=att_in.at[i, head],
+            send_sem=att_send.at[0], recv_sem=att_recv.at[i, head],
             device_id={"sp": b}, device_id_type=MESH,
         )
 
-    for t, slot in enumerate((x, across)):
-        if t:
-            x_copy(wqall.at[across]).wait_recv()
-        queries(slot)
+    def attend_far(slot, hh):
         for c in range(n_chips):
             @pl.when(chip != c)
             def _(c=c):
-                attend(c, slot)
+                attend(c, slot, (hh,))
                 for b in (2 * c, 2 * c + 1):
-                    att_copy(b, slot).start()
-    for slot in (x, across):
+                    att_copy(b, 2 * slot + hh).start()
+
+    def attend_own(slot):
         for c in range(n_chips):
             @pl.when(chip == c)
             def _(c=c):
-                attend(c, slot)
-        att_copy(partner, slot).start()
+                attend(c, slot, (0, 1))
+        for hh in range(2):
+            att_copy(partner, 2 * slot + hh).start()
+
+    queries(x, 0)
+    relay(1, 0)
+    attend_far(x, 0)
+    relay(len(parts), 0)
+
+    @pl.when(at_end)
+    def _():
+        assist_send(x, 1).wait_recv()
+
+    queries(x, 1)
+    attend_far(x, 1)
+    attend_own(x)
+    for part in range(2):
+        x_copy(whead[part].at[across], part).wait_recv()
+        queries(across, part)
+        attend_far(across, part)
+    attend_own(across)
 
     wout_copy.wait()
     squares = []
-    group = 2 * pair_dim
-
-    def piece(s, slot, local):
-        if not local:
-            pltpu.make_async_remote_copy(
-                src_ref=att_in.at[s, slot], dst_ref=att_in.at[s, slot],
-                send_sem=att_send.at[0], recv_sem=att_recv.at[s, slot],
-                device_id={"sp": partner}, device_id_type=MESH,
-            ).wait_recv()
-        values = (att_out if local else att_in)[s, slot].astype(F32)
+    group = local_heads * VDIM
+
+    def piece(s, first, count, local):
+        chosen = []
+        for hh in range(count):
+            if not local:
+                pltpu.make_async_remote_copy(
+                    src_ref=att_in.at[s, first + hh], dst_ref=att_in.at[s, first + hh],
+                    send_sem=att_send.at[0], recv_sem=att_recv.at[s, first + hh],
+                    device_id={"sp": partner}, device_id_type=MESH,
+                ).wait_recv()
+            chosen.append((att_out if local else att_in)[s, first + hh])
+        values = jnp.concatenate(chosen, axis=1).astype(F32)
         squares.append(jnp.sum(values * values, axis=-1, keepdims=True))
-        at = pl.multiple_of(s * group + slot * pair_dim, pair_dim)
-        gain = ogain[pl.ds(at, pair_dim)].astype(F32).reshape(1, -1)
+        at = pl.multiple_of(s * group + first * VDIM, VDIM)
+        gain = jnp.concatenate(
+            [head_gain[s * local_heads + first + hh] for hh in range(count)], axis=1
+        )
         return jnp.dot(
-            (values * gain).astype(BF16), wout[pl.ds(at, pair_dim), :],
+            (values * gain).astype(BF16), wout[pl.ds(at, count * VDIM), :],
             preferred_element_type=F32,
         )
 
-    acc[...] = piece(i, x, True) + piece(i, across, True)
-    acc[...] += piece(partner, x, False) + piece(partner, across, False)
+    acc[...] = piece(i, 0, local_heads, True)
+    acc[...] += piece(partner, 0, local_heads, False)
     far = []
     for d in range(1, n_chips):
         far += [far_slot(d), far_slot(d) + 1 - 2 * core]
-    steps = [(s, slot) for slot in (x, across) for s in far]
-    for s, slot in steps[:-1]:
-        acc[...] += piece(s, slot, False)
+    steps = [(s, 2 * x, 2) for s in far]
+    steps += [(s, 2 * across + hh, 1) for hh in range(2) for s in far]
+    for step in steps[:-1]:
+        acc[...] += piece(*step, False)
     term = piece(*steps[-1], False)
     factor = lax.rsqrt(sum(squares[1:], squares[0]) / (n * group) + 1e-05)
     out_ref[0] = ((acc[...] + term) * factor).astype(BF16)
@@ -723,15 +793,28 @@
             src_ref=every, dst_ref=every, send_sem=gat_send.at[a], recv_sem=gat_recv.at[a, 0],
             device_id={"sp": partner}, device_id_type=MESH,
         ).wait_send()
-    for side in range(4):
-        @pl.when(sides[side][0])
-        def _(side=side):
-            pltpu.make_async_remote_copy(
-                src_ref=wqall.at[x], dst_ref=wqall.at[x],
-                send_sem=w_send.at[side], recv_sem=w_recv.at[0],
-                device_id={"dp": sides[side][1]}, device_id_type=MESH,
-            ).wait_send()
-    x_copy(wqall.at[x]).wait_send()
+    for part in range(2):
+        for side, sender in ((0, owns), (1, owns), (2, at_mid)):
+            if part == 0 or side < 2:
+                @pl.when(sender)
+                def _(side=side, part=part):
+                    pltpu.make_async_remote_copy(
+                        src_ref=whead[part].at[x], dst_ref=whead[part].at[x],
+                        send_sem=w_send.at[4 * part + side], recv_sem=w_recv.at[0],
+                        device_id={"dp": targets[side]}, device_id_type=MESH,
+                    ).wait_send()
+
+    @pl.when(assists)
+    def _():
+        assist_send(x, 1).wait_send()
+        assist_send(across, 0).wait_send()
+
+    x_copy(wqa.at[x], 0).wait_send()
+
+    @pl.when(jnp.logical_not(at_end))
+    def _():
+        x_copy(wqb.at[x], 1).wait_send()
+
     every = att_out.at[pl.ds(0, n - 1)]
     pltpu.make_async_remote_copy(
         src_ref=every, dst_ref=every, send_sem=att_send.at[0], recv_sem=att_recv.at[0, 0],
@@ -749,7 +832,7 @@
     rank = q_latent.shape[2]
     width = w_query.shape[1]
     local_heads = H // n
-    chunks = 16
+    chunks = (8, 4)
     dim = w_out.shape[1]
     geometry = (n, columns, m // columns, chunks, local_heads)
     any_spec = pl.BlockSpec(memory_space=pl.ANY)
@@ -764,28 +847,31 @@
             pltpu.VMEM((n, rows, rank), BF16),
             pltpu.VMEM((n, rows, kv_latent.shape[2]), BF16),
             pltpu.VMEM((n, ROPE, rows), BF16),
-            pltpu.VMEM((columns, rank, width), BF16),
+            pltpu.VMEM((columns, rank, 2 * NOPE), BF16),
+            pltpu.VMEM((columns, rank, width - 2 * NOPE), BF16),
+            pltpu.VMEM((rank, width - 2 * NOPE), BF16),
             pltpu.VMEM(w_keyval.shape, BF16),
             pltpu.VMEM(w_out.shape, BF16),
             pltpu.VMEM((length, 256), F32),
             pltpu.VMEM(query_gain.shape, BF16),
             pltpu.VMEM(latent_gain.shape, BF16),
             pltpu.VMEM(out_gain.shape, BF16),
+            pltpu.VMEM((n * local_heads, 1, VDIM), F32),
             pltpu.VMEM((length, rank), BF16),
             pltpu.VMEM((columns, length, width), BF16),
             pltpu.VMEM((local_heads, length, 256), BF16),
             pltpu.VMEM((local_heads, length, 2 * VDIM), BF16),
-            pltpu.VMEM((n, columns, rows, 2 * VDIM), BF16),
-            pltpu.VMEM((n, columns, rows, 2 * VDIM), BF16),
+            pltpu.VMEM((n, local_heads, rows, VDIM), BF16),
+            pltpu.VMEM((n, local_heads, rows, VDIM), BF16),
             pltpu.VMEM((rows, dim), F32),
-            dma((10,)),
+            dma((12,)),
             dma((3,)),
             dma((3, n)),
-            dma((5,)),
-            dma((chunks,)),
+            dma((12,)),
+            dma((sum(chunks),)),
+            dma((3,)),
             dma((1,)),
-            dma((1,)),
-            dma((n, columns)),
+            dma((n, local_heads)),
         ],
         compiler_params=pltpu.CompilerParams(
             collective_id=0, has_side_effects=True, vmem_limit_bytes=56 * 1024 * 1024
@@ -819,7 +905,7 @@
     groups = k if k == columns == 2 and width % HEAD == 0 else 1
     dim = w_out.shape[1]
     group = local_heads * VDIM
-    if groups == columns and width == 2 * HEAD and H % m == 0 and m == n * columns:
+    if groups == columns and width == 2 * HEAD and H % m == 0 and n == 4 and m == n * columns:
         return paired(
             mesh, columns, q_latent, kv_latent, rope_key, w_query, w_keyval, w_out, query_gain,
             latent_gain, out_gain,

time: 28.5 us -> 26.1 us (0.916)
  Pallas kernels: 27.6 us -> 25.2 us
    pallas_call x1, Pallas kernels: 27.6 us -> 25.2 us  [paired(): pl.pallas_call(functools.partial(paired_kernel, geometry), out_shape=pltp...]
where the time goes in v3:
time: 26.1 us; the launch traced here: 26 us
  Pallas kernels  25.2 us (97%)
  local copies, waits for them, and re-layouts  0.8 us (3%)
    pallas_call x1, Pallas kernels, paired(): pl.pallas_call(functools.partial(paired_kernel, geometry), out_shape=pltp...  25.2 us
    unnamed x1, local copies, waits for them, and re-layouts  0.8 us

profile of v3, /device:TPU:0, one launch (start us, length us, event | category | flops | bytes accessed | tf_op | source)
XLA Modules:
  0.0 26.0 jit_solution(18285722735758896523)
XLA Ops:
  0.0 25.2 %shard_map.100 = bf16[1,128,2048]{2,1,0:T(8,128)(2,1)S(1)} custom-call(bf16[1,128,512]{2,1,0:T(8,128)(2,1)} %q_ref.1, bf16[1,128,512]{2,1,0:T(8,128)(2,1)} %kv_ref.1, bf16[1,64,128]{2,1,0:T(8,128)(2,1)} %bitcast.1, bf16[512,384]{1,0:T(8,128)(2,1)} %wq_ref.1, bf16[512,1024]{1,0:T(8,128)(2,1)} %wkv_ref.1, bf16[2048,2048]{1,0:T(8,128)(2,1)} %wout_ref.1, ...), custom_call_target="tpu_custom_call" | custom-call | tf_op jit(solution)/shard_map/pallas_call | solution.py:841
  25.2 0.8 %copy.12 = bf16[1,128,2048]{2,1,0:T(8,128)(2,1)} copy(bf16[1,128,2048]{2,1,0:T(8,128)(2,1)S(1)} %shard_map.100) | data formatting | bytes 1048576

commit v4 on v3

--- a/solution.py
+++ b/solution.py
@@ -430,6 +430,16 @@
         for a, (src, dst) in enumerate(((qg_ref, qgain), (lg_ref, lgain), (og_ref, ogain)))
     ]
 
+    @pl.when(z == i)
+    def _():
+        for copy in wq_copies:
+            copy.start()
+
+    for copy in own_copies:
+        copy.start()
+    for copy in gain_copies:
+        copy.start()
+
     assist_copy = pltpu.make_async_copy(
         wq_ref.at[:, first_width:first_width + wqb.shape[2]], assist, local_sem.at[11]
     )
@@ -470,18 +480,8 @@
     def _():
         assist_copy.start()
 
-    @pl.when(owns)
-    def _():
-        for copy in wq_copies:
-            copy.start()
-
-    for copy in own_copies:
-        copy.start()
-    for copy in gain_copies:
-        copy.start()
     wkv_copy.start()
     table_copy.start()
-    wout_copy.start()
 
     for h in range(local_heads):
         vs[h, :, VDIM:2 * VDIM] = jnp.ones((vs.shape[1], VDIM), BF16)
@@ -500,7 +500,7 @@
 
     def assist_send(column, sem):
         return pltpu.make_async_remote_copy(
-            src_ref=assist, dst_ref=wqb.at[x], send_sem=w_send.at[10 + sem],
+            src_ref=assist, dst_ref=wqb.at[x], send_sem=w_send.at[4],
             recv_sem=x_recv.at[1 + sem],
             device_id={"sp": twin, "dp": row(twin_end, column)}, device_id_type=MESH,
         )
@@ -508,19 +508,20 @@
     def w_copy(side, c):
         part = w_part(c)
         return pltpu.make_async_remote_copy(
-            src_ref=part, dst_ref=part, send_sem=w_send.at[4 * parts[c][0] + side], recv_sem=w_recv.at[c],
+            src_ref=part, dst_ref=part, send_sem=w_send.at[parts[c][0]], recv_sem=w_recv.at[c],
             device_id={"dp": targets[side]}, device_id_type=MESH,
         )
 
     def x_copy(source, part):
         return pltpu.make_async_remote_copy(
-            src_ref=source, dst_ref=source, send_sem=w_send.at[8 + part], recv_sem=x_recv.at[part],
+            src_ref=source, dst_ref=source, send_sem=w_send.at[2 + part], recv_sem=x_recv.at[part],
             device_id={"dp": j + 1 - 2 * x}, device_id_type=MESH,
         )
 
-    late = at_end
-    soon = at_mid | at_other
-    chunks_left = {True: list(range(len(parts))), False: list(range(len(parts)))}
+    inner_owner = (zo != 0) & (zo != Z - 1)
+    roles = (at_mid | (at_other & jnp.logical_not(inner_owner)), at_other & inner_owner, at_end)
+    chunks_left = [list(range(len(parts))) for _ in roles]
+    chunks_left[2] = chunks_left[2][:chunks[0]]
 
     def relay_one(index):
         w_copy(0, index).wait_recv()
@@ -530,37 +531,35 @@
                 w_copy(2, index).start()
         x_copy(w_part(index), parts[index][0]).start()
 
-    chunks_left[True] = chunks_left[True][:chunks[0]]
-
-    def relay(early, after):
-        for is_late, number in ((False, early), (True, after)):
-            left = chunks_left[is_late]
+    def relay(*numbers):
+        for role, number, left in zip(roles, numbers, chunks_left):
             todo = [left.pop(0) for _ in range(min(number, len(left)))]
             if todo:
-                @pl.when(late if is_late else soon)
+                @pl.when(role)
                 def _(todo=todo):
                     for index in todo:
                         relay_one(index)
 
-    def gather_copy(a, slot, target):
+    def peer(slot, reader):
+        return lax.rem(slot - reader + n, n) - 1
+
+    def gather_copy(a, slot, target, reader=None):
         dst = gathered[a][1]
         return pltpu.make_async_remote_copy(
-            src_ref=dst.at[slot], dst_ref=dst.at[slot],
-            send_sem=gat_send.at[a], recv_sem=gat_recv.at[a, slot],
+            src_ref=dst.at[slot], dst_ref=dst.at[slot], send_sem=gat_send.at[a],
+            recv_sem=gat_recv.at[a, peer(slot, target if reader is None else reader)],
             device_id={"sp": target}, device_id_type=MESH,
         )
 
     def far_slot(d):
         return 2 * lax.rem(chip + n_chips - d, n_chips) + core
 
+    def arrive(a, slot):
+        gather_copy(a, slot, partner, i).wait_recv()
+
     def forward(a, d):
-        slot = far_slot(d)
-        copy = gather_copy(a, slot, partner)
-        copy.wait_recv()
-        copy.start()
-
-    def arrive(a, slot):
-        gather_copy(a, slot, partner).wait_recv()
+        arrive(a, far_slot(d))
+        gather_copy(a, far_slot(d), partner).start()
 
     lane = lax.broadcasted_iota(jnp.int32, (rows, 128), 1)
     left = lane < 64
@@ -598,36 +597,38 @@
         at = pl.ds(pl.multiple_of(slot * rows, rows), rows)
         qn[at, :] = scaled_rows(qall[slot], qgain[...].astype(F32).reshape(1, -1))
 
+    @pl.when(owns)
+    def _():
+        for copy in wq_copies:
+            copy.wait()
+
     for copy in own_copies:
         copy.wait()
+
+    pl.semaphore_wait(barrier, count)
+
+    for a in range(3):
+        for d in range(1, n_chips):
+            gather_copy(a, i, 2 * lax.rem(chip + d, n_chips) + core).start()
+
+    @pl.when(owns)
+    def _():
+        for part in range(2):
+            x_copy(whead[part].at[x], part).start()
+        for index in range(len(parts)):
+            w_copy(1, index).start()
+            w_copy(0, index).start()
+
+    for a in range(3):
+        gather_copy(a, i, partner).start()
+
+    wout_copy.start()
     for copy in gain_copies:
         copy.wait()
     query_rows(i)
     every_gain = ogain[...].astype(F32).reshape(1, -1)
     for h in range(n * local_heads):
         head_gain[h] = every_gain[:, h * VDIM:(h + 1) * VDIM]
-
-    @pl.when(owns)
-    def _():
-        for copy in wq_copies:
-            copy.wait()
-
-    pl.semaphore_wait(barrier, count)
-
-    for a in range(3):
-        for d in range(1, n_chips):
-            gather_copy(a, i, 2 * lax.rem(chip + d, n_chips) + core).start()
-
-    @pl.when(owns)
-    def _():
-        for part in range(2):
-            x_copy(whead[part].at[x], part).start()
-        for index in range(len(parts)):
-            w_copy(1, index).start()
-            w_copy(0, index).start()
-
-    for a in range(3):
-        gather_copy(a, i, partner).start()
 
     wkv_copy.wait()
     table_copy.wait()
@@ -637,50 +638,52 @@
     keyval(partner)
     arrive(2, partner)
     query_rows(partner)
-    relay(4, 0)
+    relay(8, 12, 0)
     for d in range(1, n_chips):
         forward(0, d)
         forward(1, d)
-        relay(1, 0)
+        relay(1, 2, 0)
         keyval(far_slot(d))
+
     @pl.when(assists)
     def _():
         assist_copy.wait()
         assist_send(x, 1).start()
 
-    relay(1, 1)
+    relay(2, 2, 2)
     for d in range(1, n_chips):
         other = far_slot(d) + 1 - 2 * core
         arrive(0, other)
         arrive(1, other)
         keyval(other)
+
     @pl.when(assists)
     def _():
         assist_send(across, 0).start()
 
-    relay(1, 2)
+    relay(5, 1, 4)
     for d in range(1, n_chips):
         forward(2, d)
         query_rows(far_slot(d))
-    relay(1, 1)
+    relay(0, 1, 4)
     for d in range(1, n_chips):
         other = far_slot(d) + 1 - 2 * core
         arrive(2, other)
         query_rows(other)
-    relay(1, 5)
-
-    wide = (qn.shape[0], 128)
-    wide_left = lax.broadcasted_iota(jnp.int32, wide, 1) < 64
-
-    def queries(slot, part):
-        raw = jnp.dot(qn[...], whead[part][slot], preferred_element_type=F32)
+    relay(1, 2, chunks[0])
+
+    wide_left = lax.broadcasted_iota(jnp.int32, (2 * rows, 128), 1) < 64
+
+    def queries(slot, part, c):
+        at = pl.ds(c * 2 * rows, 2 * rows)
+        raw = jnp.dot(qn[at, :], whead[part][slot], preferred_element_type=F32)
         last = raw[:, raw.shape[1] - 128:]
-        turned = turned_pair(last, pl.ds(0, qn.shape[0]))
+        turned = turned_pair(last, at)
         if part == 0:
-            qs[slot, :, 0:128] = raw[:, 0:128].astype(BF16)
-            qs[slot, :, 128:256] = jnp.where(wide_left, turned, last).astype(BF16)
+            qs[slot, at, 0:128] = raw[:, 0:128].astype(BF16)
+            qs[slot, at, 128:256] = jnp.where(wide_left, turned, last).astype(BF16)
         else:
-            qs[slot, :, 256:384] = jnp.where(wide_left, last, turned).astype(BF16)
+            qs[slot, at, 256:384] = jnp.where(wide_left, last, turned).astype(BF16)
 
     power = HEAD ** (-0.5) * float(np.log2(np.e))
     block = 2 * rows
@@ -711,80 +714,78 @@
     def att_copy(b, head):
         return pltpu.make_async_remote_copy(
             src_ref=att_out.at[b, head], dst_ref=att_in.at[i, head],
-            send_sem=att_send.at[0], recv_sem=att_recv.at[i, head],
+            send_sem=att_send.at[0], recv_sem=att_recv.at[peer(i, b), head],
             device_id={"sp": b}, device_id_type=MESH,
         )
 
-    def attend_far(slot, hh):
+    def far_head(slot, hh):
         for c in range(n_chips):
             @pl.when(chip != c)
             def _(c=c):
+                queries(slot, hh, c)
                 attend(c, slot, (hh,))
                 for b in (2 * c, 2 * c + 1):
                     att_copy(b, 2 * slot + hh).start()
 
-    def attend_own(slot):
+    def own_heads(slot):
         for c in range(n_chips):
             @pl.when(chip == c)
             def _(c=c):
+                for hh in range(2):
+                    queries(slot, hh, c)
                 attend(c, slot, (0, 1))
         for hh in range(2):
             att_copy(partner, 2 * slot + hh).start()
 
-    queries(x, 0)
-    relay(1, 0)
-    attend_far(x, 0)
-    relay(len(parts), 0)
+    far_head(x, 0)
+    relay(len(parts), len(parts), 0)
 
     @pl.when(at_end)
     def _():
         assist_send(x, 1).wait_recv()
 
-    queries(x, 1)
-    attend_far(x, 1)
-    attend_own(x)
+    far_head(x, 1)
+    own_heads(x)
     for part in range(2):
         x_copy(whead[part].at[across], part).wait_recv()
-        queries(across, part)
-        attend_far(across, part)
-    attend_own(across)
+        far_head(across, part)
+    own_heads(across)
 
     wout_copy.wait()
     squares = []
     group = local_heads * VDIM
 
-    def piece(s, first, count, local):
-        chosen = []
-        for hh in range(count):
-            if not local:
-                pltpu.make_async_remote_copy(
-                    src_ref=att_in.at[s, first + hh], dst_ref=att_in.at[s, first + hh],
-                    send_sem=att_send.at[0], recv_sem=att_recv.at[s, first + hh],
-                    device_id={"sp": partner}, device_id_type=MESH,
-                ).wait_recv()
-            chosen.append((att_out if local else att_in)[s, first + hh])
-        values = jnp.concatenate(chosen, axis=1).astype(F32)
-        squares.append(jnp.sum(values * values, axis=-1, keepdims=True))
-        at = pl.multiple_of(s * group + first * VDIM, VDIM)
-        gain = jnp.concatenate(
-            [head_gain[s * local_heads + first + hh] for hh in range(count)], axis=1
-        )
+    def product(pieces):
+        sides = []
+        for s, first, number in pieces:
+            values = []
+            for hh in range(number):
+                if s is not i:
+                    pltpu.make_async_remote_copy(
+                        src_ref=att_in.at[s, first + hh], dst_ref=att_in.at[s, first + hh],
+                        send_sem=att_send.at[0], recv_sem=att_recv.at[peer(s, i), first + hh],
+                        device_id={"sp": partner}, device_id_type=MESH,
+                    ).wait_recv()
+                value = (att_out if s is i else att_in)[s, first + hh].astype(F32)
+                squares.append(value * value)
+                values.append((value * head_gain[s * local_heads + first + hh]).astype(BF16))
+            at = pl.multiple_of(s * group + first * VDIM, VDIM)
+            sides.append((values, wout[pl.ds(at, number * VDIM), :]))
         return jnp.dot(
-            (values * gain).astype(BF16), wout[pl.ds(at, count * VDIM), :],
+            jnp.concatenate(sum((values for values, _ in sides), []), axis=1),
+            jnp.concatenate([rows_of for _, rows_of in sides], axis=0),
             preferred_element_type=F32,
         )
 
-    acc[...] = piece(i, 0, local_heads, True)
-    acc[...] += piece(partner, 0, local_heads, False)
     far = []
     for d in range(1, n_chips):
         far += [far_slot(d), far_slot(d) + 1 - 2 * core]
-    steps = [(s, 2 * x, 2) for s in far]
-    steps += [(s, 2 * across + hh, 1) for hh in range(2) for s in far]
-    for step in steps[:-1]:
-        acc[...] += piece(*step, False)
-    term = piece(*steps[-1], False)
-    factor = lax.rsqrt(sum(squares[1:], squares[0]) / (n * group) + 1e-05)
+    acc[...] = product([(i, 0, local_heads), (partner, 0, local_heads)])
+    acc[...] += product([(s, 2 * x, 2) for s in far])
+    acc[...] += product([(s, 2 * across, 1) for s in far])
+    term = product([(s, 2 * across + 1, 1) for s in far])
+    squared = jnp.sum(sum(squares[1:], squares[0]), axis=-1, keepdims=True)
+    factor = lax.rsqrt(squared / (n * group) + 1e-05)
     out_ref[0] = ((acc[...] + term) * factor).astype(BF16)
 
     for a in range(3):
@@ -793,21 +794,24 @@
             src_ref=every, dst_ref=every, send_sem=gat_send.at[a], recv_sem=gat_recv.at[a, 0],
             device_id={"sp": partner}, device_id_type=MESH,
         ).wait_send()
-    for part in range(2):
-        for side, sender in ((0, owns), (1, owns), (2, at_mid)):
-            if part == 0 or side < 2:
-                @pl.when(sender)
-                def _(side=side, part=part):
-                    pltpu.make_async_remote_copy(
-                        src_ref=whead[part].at[x], dst_ref=whead[part].at[x],
-                        send_sem=w_send.at[4 * part + side], recv_sem=w_recv.at[0],
-                        device_id={"dp": targets[side]}, device_id_type=MESH,
-                    ).wait_send()
+    def all_sent(every, sem):
+        pltpu.make_async_remote_copy(
+            src_ref=every, dst_ref=every, send_sem=w_send.at[sem], recv_sem=w_recv.at[0],
+            device_id={"dp": targets[0]}, device_id_type=MESH,
+        ).wait_send()
+
+    @pl.when(owns)
+    def _():
+        all_sent(wqa, 0)
+        all_sent(wqb, 1)
+
+    @pl.when(at_mid)
+    def _():
+        all_sent(wqa.at[x], 0)
 
     @pl.when(assists)
     def _():
-        assist_send(x, 1).wait_send()
-        assist_send(across, 0).wait_send()
+        all_sent(wqb, 4)
 
     x_copy(wqa.at[x], 0).wait_send()
 
@@ -832,7 +836,7 @@
     rank = q_latent.shape[2]
     width = w_query.shape[1]
     local_heads = H // n
-    chunks = (8, 4)
+    chunks = (16, 4)
     dim = w_out.shape[1]
     geometry = (n, columns, m // columns, chunks, local_heads)
     any_spec = pl.BlockSpec(memory_space=pl.ANY)
@@ -866,12 +870,12 @@
             pltpu.VMEM((rows, dim), F32),
             dma((12,)),
             dma((3,)),
-            dma((3, n)),
-            dma((12,)),
+            dma((3, n - 1)),
+            dma((5,)),
             dma((sum(chunks),)),
             dma((3,)),
             dma((1,)),
-            dma((n, local_heads)),
+            dma((n - 1, local_heads)),
         ],
         compiler_params=pltpu.CompilerParams(
             collective_id=0, has_side_effects=True, vmem_limit_bytes=56 * 1024 * 1024

time: 26.1 us -> 25.2 us (0.966)
  Pallas kernels: 25.2 us -> 24.2 us
    pallas_call x1, Pallas kernels: 25.2 us -> 24.2 us  [paired(): pl.pallas_call(functools.partial(paired_kernel, geometry), out_shape=pltp...]
where the time goes in v4:
time: 25.2 us; the launch traced here: 25 us
  Pallas kernels  24.2 us (96%)
  local copies, waits for them, and re-layouts  0.8 us (3%)
    pallas_call x1, Pallas kernels, paired(): pl.pallas_call(functools.partial(paired_kernel, geometry), out_shape=pltp...  24.2 us
    unnamed x1, local copies, waits for them, and re-layouts  0.8 us

profile of v4, /device:TPU:0, one launch (start us, length us, event | category | flops | bytes accessed | tf_op | source)
XLA Modules:
  0.0 25.0 jit_solution(14888512506586186375)
XLA Ops:
  0.0 24.2 %shard_map.100 = bf16[1,128,2048]{2,1,0:T(8,128)(2,1)S(1)} custom-call(bf16[1,128,512]{2,1,0:T(8,128)(2,1)} %q_ref.1, bf16[1,128,512]{2,1,0:T(8,128)(2,1)} %kv_ref.1, bf16[1,64,128]{2,1,0:T(8,128)(2,1)} %bitcast.1, bf16[512,384]{1,0:T(8,128)(2,1)} %wq_ref.1, bf16[512,1024]{1,0:T(8,128)(2,1)} %wkv_ref.1, bf16[2048,2048]{1,0:T(8,128)(2,1)} %wout_ref.1, ...), custom_call_target="tpu_custom_call" | custom-call | tf_op jit(solution)/shard_map/pallas_call | solution.py:845
  24.2 0.8 %copy.12 = bf16[1,128,2048]{2,1,0:T(8,128)(2,1)} copy(bf16[1,128,2048]{2,1,0:T(8,128)(2,1)S(1)} %shard_map.100) | data formatting | bytes 1048576
